TPU v7x, 32 devices: a whole 2x2x4 slice. The times are simulated.
32 devices in a mesh: kv: 8 (over z, x), tp: 4 (over y, core).
Axes of the slice: x: 2, y: 2, z: 4, core: 2. Of those that a mesh axis runs over, the one named last changes fastest.
Arguments:
- tokens: bfloat16 [64, 4, 4096], P(None, None, 'kv')
- norm_gain: float32 [4096], replicated, may hold values from 0.1 to 1.9
- w_query: bfloat16 [4096, 4096], P('kv', 'tp'), may hold values from -0.09375 to 0.09375
- w_key: bfloat16 [4096, 4096], P('kv', 'tp'), may hold values from -0.09375 to 0.09375
- w_value: bfloat16 [4096, 4096], P('kv', 'tp'), may hold values from -0.09375 to 0.09375
- w_gate: bfloat16 [4096, 4096], P('kv', 'tp'), may hold values from -0.09375 to 0.09375
- w_decay: bfloat16 [4096, 32], replicated, may hold values from -0.09375 to 0.09375
- w_beta: bfloat16 [4096, 32], replicated, may hold values from -0.09375 to 0.09375
- decay_rate: float32 [32], replicated, may hold values from 0.02 to 3
- head_gain: float32 [128], replicated, may hold values from 0.1 to 1.9
- w_out: bfloat16 [4096, 4096], P('tp', 'kv'), may hold values from -0.09375 to 0.09375
- state: float32 [64, 32, 128, 128], P('kv', 'tp'), may hold values from -0.4 to 0.4
- prev_keys: bfloat16 [64, 32, 4, 128], P('kv', 'tp'), may hold values from -6 to 6
- prev_values: bfloat16 [64, 32, 4, 128], P('kv', 'tp'), may hold values from -6 to 6
- prev_log_decay: float32 [64, 32, 4], P('kv', 'tp'), may hold values from -0.7 to -0.02
- prev_beta: float32 [64, 32, 4], P('kv', 'tp'), may hold values from 0.1 to 0.9
- accepted: int32 [64], P('kv'), may hold values from 0 to 4
Outputs:
- mixed: bfloat16 [64, 4, 4096], P('tp', None, 'kv')
- carried: float32 [64, 32, 128, 128], P('kv', 'tp')
All inputs are finite; a program needn't handle non-finite values.
Results may differ from a plain program's by a relative error of at most 0.0069.
Values may be sent and summed in bfloat16 or wider, within the bound.
A program may use at most 128 MiB of HBM per device.

v0:
```python
import jax
import jax.numpy as jnp
from jax import lax
from jax.sharding import PartitionSpec as P

epsilon = 1e-06


def unit_rows(values):
    return values * lax.rsqrt(jnp.sum(values * values, axis=-1, keepdims=True) + epsilon)


def apply_update(matrix, keyvec, valvec, logd, strength):
    decayed = jnp.exp(logd)[..., None, None] * matrix
    predicted = jnp.einsum("bhde,bhd->bhe", decayed, keyvec, precision=lax.Precision.HIGHEST)
    change = strength[..., None] * (valvec - predicted)
    return decayed + jnp.einsum("bhd,bhe->bhde", keyvec, change, precision=lax.Precision.HIGHEST)


def per_device(
    tokens,
    norm_gain,
    w_query,
    w_key,
    w_value,
    w_gate,
    w_decay,
    w_beta,
    decay_rate,
    head_gain,
    w_out,
    state,
    prev_keys,
    prev_values,
    prev_log_decay,
    prev_beta,
    accepted,
):
    f32 = jnp.float32
    seq_here, heads_here, key_size, value_size = state.shape
    props = tokens.shape[1]
    width_here = tokens.shape[2]
    dmodel = w_decay.shape[0]
    head_start = lax.axis_index("tp") * heads_here
    decay_cols = lax.dynamic_slice_in_dim(w_decay, head_start, heads_here, 1)
    beta_cols = lax.dynamic_slice_in_dim(w_beta, head_start, heads_here, 1)
    rate_here = lax.dynamic_slice_in_dim(decay_rate, head_start, heads_here, 0)
    qwidth = heads_here * key_size
    vwidth = heads_here * value_size
    features = tokens.reshape(-1, width_here).astype(f32)
    total_sq = lax.psum(jnp.sum(features * features, axis=1), "kv")
    scale = lax.rsqrt(total_sq / dmodel + epsilon)[:, None]
    row_start = lax.axis_index("kv") * width_here
    gain_part = lax.dynamic_slice_in_dim(norm_gain, row_start, width_here, 0)
    normed = (features * scale * gain_part).astype(jnp.bfloat16)
    joined = jnp.concatenate(
        [
            w_query,
            w_key,
            w_value,
            w_gate,
            lax.dynamic_slice_in_dim(decay_cols, row_start, width_here, 0),
            lax.dynamic_slice_in_dim(beta_cols, row_start, width_here, 0),
        ],
        axis=1,
    )
    summed = lax.psum_scatter(
        jnp.dot(normed, joined, preferred_element_type=f32), "kv", scatter_dimension=0, tiled=True
    )
    qraw = summed[:, :qwidth]
    kraw = summed[:, qwidth : 2 * qwidth]
    vraw = summed[:, 2 * qwidth : 2 * qwidth + vwidth]
    zraw = summed[:, 2 * qwidth + vwidth : 2 * qwidth + 2 * vwidth]
    araw = summed[:, 2 * qwidth + 2 * vwidth : 2 * qwidth + 2 * vwidth + heads_here]
    braw = summed[:, 2 * qwidth + 2 * vwidth + heads_here :]
    query = unit_rows(
        jax.nn.silu(qraw).reshape(seq_here, props, heads_here, key_size)
    ) * key_size ** (-0.5)
    keyrow = unit_rows(jax.nn.silu(kraw).reshape(seq_here, props, heads_here, key_size))
    value = jax.nn.silu(vraw).reshape(seq_here, props, heads_here, value_size)
    beta = jax.nn.sigmoid(braw).reshape(seq_here, props, heads_here)
    logdecay = (-rate_here * jax.nn.softplus(araw)).reshape(seq_here, props, heads_here)
    old_keys = unit_rows(prev_keys.astype(f32))
    old_values = prev_values.astype(f32)
    matrix = state
    for proposal in range(props):
        keep = (proposal < accepted).astype(f32)[:, None]
        matrix = apply_update(
            matrix,
            old_keys[:, :, proposal],
            old_values[:, :, proposal],
            prev_log_decay[:, :, proposal] * keep,
            prev_beta[:, :, proposal] * keep,
        )
    carried = matrix
    results = []
    for proposal in range(props):
        matrix = apply_update(
            matrix,
            keyrow[:, proposal],
            value[:, proposal],
            logdecay[:, proposal],
            beta[:, proposal],
        )
        results.append(
            jnp.einsum("bhde,bhd->bhe", matrix, query[:, proposal], precision=lax.Precision.HIGHEST)
        )
    attended = jnp.stack(results, axis=1)
    zgate = zraw.reshape(seq_here, props, heads_here, value_size)
    headout = attended * lax.rsqrt(jnp.mean(attended * attended, axis=-1, keepdims=True) + epsilon)
    headout = (
        (headout * head_gain * jax.nn.silu(zgate))
        .astype(jnp.bfloat16)
        .reshape(seq_here * props, vwidth)
    )
    terms = jnp.dot(
        lax.all_gather(headout, "kv", axis=0, tiled=True), w_out, preferred_element_type=f32
    )
    mixed = lax.psum_scatter(terms, "tp", scatter_dimension=0, tiled=True)
    return (mixed.reshape(-1, props, width_here).astype(jnp.bfloat16), carried)


def solution(mesh):
    placed = (
        P(None, None, "kv"),
        P(),
        P("kv", "tp"),
        P("kv", "tp"),
        P("kv", "tp"),
        P("kv", "tp"),
        P(),
        P(),
        P(),
        P(),
        P("tp", "kv"),
        P("kv", "tp", None, None),
        P("kv", "tp", None, None),
        P("kv", "tp", None, None),
        P("kv", "tp", None),
        P("kv", "tp", None),
        P("kv"),
    )
    return jax.shard_map(
        per_device,
        mesh=mesh,
        in_specs=placed,
        out_specs=(P("tp", None, "kv"), P("kv", "tp", None, None)),
        check_vma=False,
    )
```

profile of v0, /device:TPU:1, one launch (start us, length us, event | category | flops | bytes accessed | tf_op | source)
XLA Modules:
  0.0 254.2 jit_solution(14906130394573338317)
XLA Ops:
  7.2 0.0 copy-start
  7.2 0.0 reduce-scatter.3.cloned.1.call-start
  7.2 1.1 reshape.198
  8.3 1.2 multiply_reduce_fusion
  9.5 0.8 dynamic_slice.16
  10.3 0.2 copy.37
  10.5 0.8 dynamic_slice.17
  11.3 0.2 copy.38
  11.4 0.8 dynamic_slice.15
  12.2 0.1 reduce_sum.48
  12.3 18.7 %psum.7 = f32[256]{0:T(256)S(1)} all-reduce(f32[256]{0:T(256)S(1)} %reduce_sum.48), channel_id=1, replica_groups=mesh['kv'=8,'tp'=4] {'kv'}, use_global_device_ids=true, to_apply=%region_1.0 | all-reduce | flops 256 | bytes 2048 | tf_op jit(solution)/shard_map/psum | solution.py:51
  31.0 7.6 %concatenate.3 = bf16[512,4112]{1,0:T(8,128)(2,1)} concatenate(bf16[512,1024]{1,0:T(8,128)(2,1)} %param.19, bf16[512,1024]{1,0:T(8,128)(2,1)} %param.20, bf16[512,1024]{1,0:T(8,128)(2,1)} %param.21, bf16[512,1024]{1,0:T(8,128)(2,1)} %param.22, bf16[512,8]{1,0:T(8,128)(2,1)S(1)} %copy.37, bf16[512,8]{1,0:T(8,128)(2,1)S(1)} %copy.38), dimensions={1} | concatenate | bytes 8421376 | tf_op jit(solution)/shard_map/concatenate | solution.py:56
  38.6 5.6 %fusion.51 = f32[256,4112]{1,0:T(8,128)} fusion(bf16[512,4112]{1,0:T(8,128)(2,1)} %concatenate.3, f32[256,512]{1,0:T(8,128)S(1)} %reshape.198, f32[512]{0:T(512)S(1)} %dynamic_slice.15, f32[256]{0:T(256)S(1)} %add_rsqrt_fusion.4), kind=kOutput, calls=%fused_computation.60 | convolution fusion | flops 1078329344 | bytes 8948736 | tf_op jit(solution)/shard_map/dot_general | solution.py:68
  44.3 0.0 copy-start.4
  44.3 0.0 reduce-scatter.3.cloned.1.call-update
  44.3 0.0 reduce-scatter.5.cloned.1.call-start
  44.3 0.5 copy-done.9
  44.9 0.1 dynamic-slice_negate_fusion
  45.0 0.1 copy-done.3
  45.1 0.1 fusion.54
  45.3 0.1 multiply_exponential_fusion
  45.4 0.1 multiply_bitcast_fusion.5
  45.5 0.1 multiply_exponential_fusion.2
  45.6 0.1 multiply_bitcast_fusion.3
  45.7 0.1 fusion.81
  45.8 0.1 convert_multiply_fusion
  45.9 5.8 %fusion.12 = f32[8,8,1,128]{3,2,1,0:T(1,128)S(1)} fusion(f32[8,8,128,128]{3,2,1,0:T(8,128)} %param.28, f32[8,8]{1,0:T(8,128)S(1)} %get-tuple-element.51, f32[8,8,4,128]{3,2,1,0:T(4,128)S(1)} %convert_multiply_fusion), kind=kOutput, calls=%fused_computation.19 | convolution fusion | flops 13631488 | bytes 4263936 | tf_op jit(solution)/shard_map/bhde,bhd->bhe/dot_general | solution.py:15
  51.7 0.1 subtract_multiply_fusion.3
  51.8 0.1 fusion.80
  51.9 4.3 %fusion.50 = f32[8,8,1,128]{3,2,1,0:T(1,128)S(1)} fusion(f32[8,8,128,128]{3,2,1,0:T(8,128)S(1)} %copy-done.2, f32[8,8,128]{2,1,0:T(8,128)S(1)} %subtract_multiply_fusion.3, f32[8,8,128]{2,1,0:T(8,128)S(1)} %bitcast.220, f32[8,8]{1,0:T(8,128)S(1)} %get-tuple-element.51, f32[8,8]{1,0:T(8,128)S(1)} %get-tuple-element.52, ...), kind=kOutput, calls=%fused_computation.57 | convolution fusion | flops 16777216 | bytes 4333568 | tf_op jit(solution)/shard_map/bhde,bhd->bhe/dot_general | solution.py:15
  56.2 0.1 subtract_multiply_fusion.2
  56.3 5.8 %fusion.14 = f32[8,8,1,128]{3,2,1,0:T(1,128)S(1)} fusion(f32[8,8,128]{2,1,0:T(8,128)S(1)} %subtract_multiply_fusion.2, f32[8,8,128]{2,1,0:T(8,128)S(1)} %bitcast.217, f32[8,8]{1,0:T(8,128)S(1)} %get-tuple-element.53, f32[8,8,128,128]{3,2,1,0:T(8,128)S(1)} %copy-done.2, f32[8,8,128]{2,1,0:T(8,128)S(1)} %subtract_multiply_fusion.3, ...), kind=kOutput, calls=%fused_computation.21 | convolution fusion | flops 19922944 | bytes 4403200 | tf_op jit(solution)/shard_map/bhde,bhd->bhe/dot_general | solution.py:15
  62.1 0.1 subtract_multiply_fusion.1
  62.2 7.7 %fusion.15 = f32[8,8,1,128]{3,2,1,0:T(1,128)S(1)} fusion(f32[8,8,128]{2,1,0:T(8,128)S(1)} %subtract_multiply_fusion.1, f32[8,8,128]{2,1,0:T(8,128)S(1)} %bitcast.215, f32[8,8,128]{2,1,0:T(8,128)S(1)} %subtract_multiply_fusion.2, f32[8,8,128]{2,1,0:T(8,128)S(1)} %bitcast.218, f32[8,8]{1,0:T(8,128)S(1)} %get-tuple-element.53, ...), kind=kOutput, calls=%fused_computation.22 | convolution fusion | flops 23068672 | bytes 4472832 | tf_op jit(solution)/shard_map/bhde,bhd->bhe/dot_general | solution.py:15
  69.9 0.1 subtract_multiply_fusion
  70.0 6.7 %multiply_add_fusion.3 = f32[8,8,128,128]{3,2,1,0:T(8,128)} fusion(f32[8,8,128]{2,1,0:T(8,128)S(1)} %subtract_multiply_fusion, f32[8,8,128]{2,1,0:T(8,128)S(1)} %bitcast.214, f32[8,8,128]{2,1,0:T(8,128)S(1)} %subtract_multiply_fusion.1, f32[8,8,128]{2,1,0:T(8,128)S(1)} %bitcast.216, f32[8,8,128]{2,1,0:T(8,128)S(1)} %subtract_multiply_fusion.2, ...), kind=kLoop, calls=%fused_computation.6 | loop fusion | flops 12582912 | bytes 8651776 | tf_op jit(solution)/shard_map/add | solution.py:17
  76.7 58.7 %reduce-scatter.3.cloned.1.call-done = f32[32,4112]{1,0:T(8,128)} async-done(((f32[256,4112]{1,0:T(8,128)}), f32[32,4112]{1,0:T(8,128)}) %reduce-scatter.3.cloned.1.call-update) | async-done | bytes 526352 | tf_op jit(solution)/shard_map/reduce_scatter | solution.py:67
  135.4 1.3 multiply_bitcast_fusion.1
  136.7 0.1 multiply_reduce_fusion.2
  136.9 0.1 multiply_multiply_fusion
  137.0 0.1 multiply_reduce_fusion.3
  137.2 0.1 broadcast_multiply_fusion
  137.3 0.9 fusion.73
  138.3 5.8 %fusion.10 = f32[8,8,1,128]{3,2,1,0:T(1,128)S(1)} fusion(f32[8,8,128,1]{2,3,1,0:T(1,128)S(1)} %bitcast.210, f32[8,8,128,128]{3,2,1,0:T(8,128)} %multiply_add_fusion.3, f32[8,8]{1,0:T(8,128)S(1)} %get-tuple-element.56), kind=kOutput, calls=%fused_computation.17 | convolution fusion | flops 13631488 | bytes 4260096 | tf_op jit(solution)/shard_map/bhde,bhd->bhe/dot_general | solution.py:15
  144.1 0.1 fusion.65
  144.2 4.1 %fusion.16 = f32[8,8,1,128]{3,2,1,0:T(1,128)S(1)} fusion(f32[8,8,128,1]{2,3,1,0:T(1,128)S(1)} %bitcast.213, f32[8,8,128,128]{3,2,1,0:T(8,128)S(1)} %copy-done.1, f32[8,8,128]{2,1,0:T(8,128)S(1)} %fusion.65, f32[8,8,128]{2,1,0:T(8,128)S(1)} %get-tuple-element.12, f32[8,8]{1,0:T(8,128)S(1)} %get-tuple-element.56), kind=kOutput, calls=%fused_computation.23 | convolution fusion | flops 15728640 | bytes 4325632 | tf_op jit(solution)/shard_map/bhde,bhd->bhe/dot_general | solution.py:106
  148.3 4.3 %fusion.8 = f32[8,8,1,128]{3,2,1,0:T(1,128)S(1)} fusion(f32[8,8,128,1]{2,3,1,0:T(1,128)S(1)} %bitcast.238, f32[8,8,128,128]{3,2,1,0:T(8,128)S(1)} %copy-done.1, f32[8,8]{1,0:T(8,128)S(1)} %get-tuple-element.55, f32[8,8,128]{2,1,0:T(8,128)S(1)} %fusion.65, f32[8,8,128]{2,1,0:T(8,128)S(1)} %get-tuple-element.12, f32[8,8]{1,0:T(8,128)S(1)} %get-tuple-element.56), kind=kOutput, calls=%fused_computation.15 | convolution fusion | flops 16777216 | bytes 4325888 | tf_op jit(solution)/shard_map/bhde,bhd->bhe/dot_general | solution.py:15
  152.5 0.1 fusion.63
  152.6 5.8 %fusion.78 = f32[8,8,1,128]{3,2,1,0:T(1,128)S(1)} fusion(f32[8,8,128,1]{2,3,1,0:T(1,128)S(1)} %bitcast.247, f32[8,8,128,128]{3,2,1,0:T(8,128)S(1)} %copy-done.1, f32[8,8,128]{2,1,0:T(8,128)S(1)} %fusion.63, f32[8,8,128]{2,1,0:T(8,128)S(1)} %get-tuple-element.13, f32[8,8]{1,0:T(8,128)S(1)} %get-tuple-element.55, f32[8,8,128]{2,1,0:T(8,128)S(1)} %fusion.65, ...), kind=kOutput, calls=%fused_computation.136 | convolution fusion | flops 18874368 | bytes 4391424 | tf_op jit(solution)/shard_map/bhde,bhd->bhe/dot_general | solution.py:106
  158.4 5.8 %fusion.6 = f32[8,8,1,128]{3,2,1,0:T(1,128)S(1)} fusion(f32[8,8,128,1]{2,3,1,0:T(1,128)S(1)} %bitcast.237, f32[8,8]{1,0:T(8,128)S(1)} %get-tuple-element.58, f32[8,8,128,128]{3,2,1,0:T(8,128)S(1)} %copy-done.1, f32[8,8,128]{2,1,0:T(8,128)S(1)} %fusion.63, f32[8,8,128]{2,1,0:T(8,128)S(1)} %get-tuple-element.13, f32[8,8]{1,0:T(8,128)S(1)} %get-tuple-element.55, ...), kind=kOutput, calls=%fused_computation.13 | convolution fusion | flops 19922944 | bytes 4391680 | tf_op jit(solution)/shard_map/bhde,bhd->bhe/dot_general | solution.py:15
  164.2 0.1 fusion.61
  164.3 7.7 %fusion.17 = f32[8,8,1,128]{3,2,1,0:T(1,128)S(1)} fusion(f32[8,8,128,1]{2,3,1,0:T(1,128)S(1)} %bitcast.246, f32[8,8,128]{2,1,0:T(8,128)S(1)} %fusion.61, f32[8,8,128]{2,1,0:T(8,128)S(1)} %get-tuple-element.14, f32[8,8]{1,0:T(8,128)S(1)} %get-tuple-element.58, f32[8,8,128,128]{3,2,1,0:T(8,128)S(1)} %copy-done.1, f32[8,8,128]{2,1,0:T(8,128)S(1)} %fusion.63, ...), kind=kOutput, calls=%fused_computation.24 | convolution fusion | flops 22020096 | bytes 4457216 | tf_op jit(solution)/shard_map/bhde,bhd->bhe/dot_general | solution.py:106
  172.0 7.7 %fusion.4 = f32[8,8,1,128]{3,2,1,0:T(1,128)S(1)} fusion(f32[8,8,128,1]{2,3,1,0:T(1,128)S(1)} %bitcast.236, f32[8,8]{1,0:T(8,128)S(1)} %get-tuple-element.57, f32[8,8,128]{2,1,0:T(8,128)S(1)} %fusion.61, f32[8,8,128]{2,1,0:T(8,128)S(1)} %get-tuple-element.14, f32[8,8]{1,0:T(8,128)S(1)} %get-tuple-element.58, f32[8,8,128,128]{3,2,1,0:T(8,128)S(1)} %copy-done.1, ...), kind=kOutput, calls=%fused_computation.11 | convolution fusion | flops 23068672 | bytes 4457472 | tf_op jit(solution)/shard_map/bhde,bhd->bhe/dot_general | solution.py:15
  179.8 0.1 fusion.59
  179.8 10.6 %fusion = f32[8,8,1,128]{3,2,1,0:T(1,128)S(1)} fusion(f32[8,8,128,1]{2,3,1,0:T(1,128)S(1)} %bitcast.245, f32[8,8,128]{2,1,0:T(8,128)S(1)} %fusion.59, f32[8,8,128]{2,1,0:T(8,128)S(1)} %get-tuple-element.11, f32[8,8]{1,0:T(8,128)S(1)} %get-tuple-element.57, f32[8,8,128]{2,1,0:T(8,128)S(1)} %fusion.61, f32[8,8,128]{2,1,0:T(8,128)S(1)} %get-tuple-element.14, ...), kind=kOutput, calls=%fused_computation | convolution fusion | flops 25165824 | bytes 4523008 | tf_op jit(solution)/shard_map/bhde,bhd->bhe/dot_general | solution.py:106
  190.4 0.1 multiply_reduce_fusion.1
  190.6 0.1 fusion.57
  190.7 1.0 fusion.56
  191.6 25.7 %all_gather.3 = bf16[256,1024]{1,0:T(8,128)(2,1)S(1)} all-gather(bf16[32,1024]{1,0:T(8,128)(2,1)S(1)} %fusion.56), channel_id=1, replica_groups=mesh['kv'=8,'tp'=4] {'kv'}, dimensions={0}, use_global_device_ids=true | all-gather | bytes 589824 | tf_op jit(solution)/shard_map/all_gather | solution.py:117
  217.3 1.3 fusion.86
  218.6 0.0 reduce-scatter.5.cloned.1.call-update
  218.6 27.2 %reduce-scatter.5.cloned.1.call-done = f32[64,512]{1,0:T(8,128)} async-done(((f32[256,512]{1,0:T(8,128)}), f32[64,512]{1,0:T(8,128)}) %reduce-scatter.5.cloned.1.call-update) | async-done | bytes 131088 | tf_op jit(solution)/shard_map/reduce_scatter | solution.py:119
  245.8 0.9 convert_element_type.51
  246.7 0.7 convert_element_type.52
  (34 shorter events, 0.3 us)
Async XLA Ops:
  7.2 210.2 %copy-start = (bf16[1024,512]{1,0:T(8,128)(2,1)S(1)}, bf16[1024,512]{1,0:T(8,128)(2,1)}, u32[]{:S(2)}) copy-start(bf16[1024,512]{1,0:T(8,128)(2,1)} %param.27) | copy-start | bytes 3145732
  7.2 128.2 %reduce-scatter.3.cloned.1.call-start = ((), (), s32[]{:S(2)}) async-start(), calls=%async_computation.2 | async-start | bytes 4866048 | tf_op jit(solution)/shard_map/reduce_scatter | solution.py:67
  44.2 0.7 copy-start.9
  44.2 0.9 copy-start.3
  44.2 1.0 copy-start.7
  44.2 1.0 copy-start.8
  44.2 1.0 copy-start.5
  44.2 1.1 copy-start.6
  44.3 1.4 copy-start.4
  44.3 201.5 %reduce-scatter.5.cloned.1.call-start = ((), (), s32[]{:S(2)}) async-start(), calls=%async_computation.3 | async-start | bytes 655360 | tf_op jit(solution)/shard_map/reduce_scatter | solution.py:119
  44.9 7.0 %copy-start.2 = (f32[8,8,128,128]{3,2,1,0:T(8,128)S(1)}, f32[8,8,128,128]{3,2,1,0:T(8,128)}, u32[]{:S(2)}) copy-start(f32[8,8,128,128]{3,2,1,0:T(8,128)} %param.28) | copy-start | bytes 12582916
  135.4 8.8 %copy-start.1 = (f32[8,8,128,128]{3,2,1,0:T(8,128)S(1)}, f32[8,8,128,128]{3,2,1,0:T(8,128)}, u32[]{:S(2)}) copy-start(f32[8,8,128,128]{3,2,1,0:T(8,128)} %multiply_add_fusion.3) | copy-start | bytes 12582916
Sparse Core Ops, SparseCore 0:
  44.4 90.9 reduce-scatter.2
  218.7 27.0 reduce-scatter.4
where the time goes:
time: 256 us; the launch traced here: 254 us
  waiting for transfers between devices  85.9 us (34%)
  matrix products  82.3 us (32%)
  blocking collectives  44.4 us (17%)
  between operations  14.4 us (6%)
  other arithmetic  13.9 us (5%)
  local copies, waits for them, and re-layouts  13.2 us (5%)
    reduce_scatter x1, waiting for transfers between devices, per_device(): lax.psum_scatter(jnp.dot(normed, joined, preferred_element_type=f32), 'kv...  58.7 us
    dot_general x8, matrix products, apply_update(): jnp.einsum('bhde,bhd->bhe', decayed, keyvec, precision=lax.Precision.HIGH...  47.3 us
    dot_general x4, matrix products, per_device(): jnp.einsum('bhde,bhd->bhe', matrix, query[:, proposal], precision=lax.Pre...  28.2 us
    reduce_scatter x1, waiting for transfers between devices, per_device(): mixed = lax.psum_scatter(terms, 'tp', scatter_dimension=0, tiled=True)  27.2 us
    all_gather x1, blocking collectives, per_device(): lax.all_gather(headout, 'kv', axis=0, tiled=True)  25.7 us
    psum x1, blocking collectives, per_device(): total_sq = lax.psum(jnp.sum(features * features, axis=1), 'kv')  18.7 us
    concatenate x1, local copies, waits for them, and re-layouts, per_device(): jnp.concatenate([w_query, w_key, w_value, w_gate, lax.dynamic_slice_in_di...  7.62 us
    add x1, other arithmetic, apply_update(): decayed + jnp.einsum('bhd,bhe->bhde', keyvec, change, precision=lax.Preci...  6.66 us
  transfers between devices with their start and end apart: 2, of which 2 were waited for; matrix products, arithmetic and copies ran while one was open for 12% of the time, Pallas kernels for 0%

commit v1 on v0

v1 whole, which is shorter than its diff:
```python
import functools

import jax
import jax.numpy as jnp
from jax import lax
from jax.experimental import pallas as pl
from jax.experimental.pallas import tpu as pltpu
from jax.sharding import PartitionSpec as P

epsilon = 1e-06
MESH = pl.DeviceIdType.MESH
f32 = jnp.float32
bf16 = jnp.bfloat16
HIGH = lax.Precision.HIGHEST


def exact_dot(a, b, dims=((1,), (0,))):
    return lax.dot_general(a, b, (dims, ((), ())), precision=HIGH, preferred_element_type=f32)


def fast_dot(a, b, dims=((1,), (0,))):
    return lax.dot_general(a, b, (dims, ((), ())), preferred_element_type=f32)


def split(a):
    high = a.astype(bf16)
    return high, (a - high.astype(f32)).astype(bf16)


def split_dot(a, b, dims=((1,), (0,))):
    ah, al = split(a)
    bh, bl = split(b)
    return fast_dot(ah, bh, dims) + (fast_dot(ah, bl, dims) + fast_dot(al, bh, dims))


def grid_ids(rows, props):
    r = lax.broadcasted_iota(jnp.int32, (rows, rows), 0)
    c = lax.broadcasted_iota(jnp.int32, (rows, rows), 1)
    return r, c, (r // props) == (c // props)


def chain(g, beta, key, props):
    rows = key.shape[0]
    r, c, same = grid_ids(rows, props)
    lower = same & (c <= r)
    g_row = jnp.sum(jnp.where(r == c, g, 0.0), axis=0, keepdims=True)
    cum = jnp.sum(jnp.where(lower, g_row, 0.0), axis=1, keepdims=True)
    cum_row = jnp.sum(jnp.where(same & (r <= c), g, 0.0), axis=0, keepdims=True)
    decay = jnp.where(lower, jnp.exp(jnp.where(lower, cum - cum_row, 0.0)), 0.0)
    after = jnp.sum(jnp.where(same & (c > r), g_row, 0.0), axis=1, keepdims=True)
    return cum, decay, after, same & (c < r)


def solve(a, rhs, props):
    power, factors, reach = a, [], 2
    while reach < props:
        power = split_dot(power, power)
        factors.append(power)
        reach *= 2
    for factor in factors[::-1]:
        rhs = rhs + split_dot(factor, rhs)
    return rhs - split_dot(a, rhs)


def spread_rows(x, groups, props):
    owner = lax.broadcasted_iota(jnp.int32, x.shape, 0)
    owner = (owner // props) % groups
    return jnp.concatenate([jnp.where(owner == i, x, jnp.zeros_like(x)) for i in range(groups)], axis=1)


def carried_kernel(state_ref, keys_ref, values_ref, logd_ref, beta_ref, acc_ref, out_ref, krow, vrow):
    seqs, heads, dk, dv = state_ref.shape
    props = keys_ref.shape[2]
    rows = heads * props
    first = pl.program_id(0) * seqs
    row4 = lax.broadcasted_iota(jnp.int32, (rows, props), 0)
    lane4 = lax.broadcasted_iota(jnp.int32, (rows, props), 1)
    pick = (row4 % props) == lane4
    rowh = lax.broadcasted_iota(jnp.int32, (rows, heads), 0)
    laneh = lax.broadcasted_iota(jnp.int32, (rows, heads), 1)
    repeat = jnp.where((rowh // props) == laneh, 1.0, 0.0)
    prop_of = lax.broadcasted_iota(jnp.int32, (rows, 1), 0) % props
    for s in range(seqs):
        for h in range(heads):
            krow[s, h * props : (h + 1) * props, :] = keys_ref[s, h].astype(f32)
            vrow[s, h * props : (h + 1) * props, :] = values_ref[s, h].astype(f32)
    for s in range(seqs):
        keep = prop_of < acc_ref[first + s]
        g = jnp.sum(jnp.where(pick, exact_dot(repeat, logd_ref[s]), 0.0), axis=1, keepdims=True)
        b = jnp.sum(jnp.where(pick, exact_dot(repeat, beta_ref[s]), 0.0), axis=1, keepdims=True)
        g = jnp.where(keep, g, 0.0)
        b = jnp.where(keep, b, 0.0)
        key = krow[s]
        key = key * lax.rsqrt(jnp.sum(key * key, axis=1, keepdims=True) + epsilon)
        value = vrow[s]
        cum, decay, after, strict = chain(g, b, key, props)
        kh, kl = split(key)
        kk = split_dot(key, key, ((1,), (1,)))
        a = jnp.where(strict, b * decay * kk, 0.0)
        st = state_ref[s].reshape(heads * dk, dv)
        both = jnp.concatenate([kh, kl], axis=0)
        seen = fast_dot(spread_rows(both, heads, props), st.astype(bf16))
        seen = seen[:rows] + seen[rows:]
        u = solve(a, b * (value - jnp.exp(cum) * seen), props) * jnp.exp(after)
        uh, ul = split(u)
        left = spread_rows(jnp.concatenate([kh, kl, kh], axis=0), heads, props)
        right = jnp.concatenate([uh, uh, ul], axis=0)
        change = fast_dot(left, right, ((0,), (0,)))
        total = jnp.exp(cum + after)
        for h in range(heads):
            out_ref[s, h] = total[h * props : h * props + 1, :] * state_ref[s, h] + change[h * dk : (h + 1) * dk]


def carried_call(state, prev_keys, prev_values, prev_log_decay, prev_beta, accepted):
    seqs, heads, dk, dv = state.shape
    props = prev_keys.shape[2]
    step = 2 if seqs % 2 == 0 else 1
    at4 = lambda i: (i, 0, 0, 0)
    at3 = lambda i: (i, 0, 0)
    return pl.pallas_call(
        carried_kernel,
        grid=(seqs // step,),
        out_shape=jax.ShapeDtypeStruct(state.shape, f32),
        in_specs=[
            pl.BlockSpec((step, heads, dk, dv), at4),
            pl.BlockSpec((step, heads, props, dk), at4),
            pl.BlockSpec((step, heads, props, dv), at4),
            pl.BlockSpec((step, heads, props), at3),
            pl.BlockSpec((step, heads, props), at3),
            pl.BlockSpec(memory_space=pltpu.SMEM),
        ],
        out_specs=pl.BlockSpec((step, heads, dk, dv), at4),
        scratch_shapes=[pltpu.VMEM((step, heads * props, dk), f32), pltpu.VMEM((step, heads * props, dv), f32)],
        cost_estimate=pl.CostEstimate(flops=2 * state.size * props, bytes_accessed=8 * state.size, transcendentals=0),
    )(state, prev_keys, prev_values, prev_log_decay, prev_beta, accepted)


def step_kernel(
    nx, nz, ntp,
    tok_ref, gain_ref, wd_hbm, wb_hbm, rate_ref, hgain_ref, wq_hbm, wk_hbm, wv_hbm, wz_hbm, wo_hbm, car_hbm,
    out_ref,
    xrow, w_v, wo_v, wd_v, wb_v, car_v, ssb, nb, xs, xr, own, zs, zr, axs, axr, aown, azs, azr, abt, gat, terms, ts, tr,
    loc, ss_s, ss_r, x_s, x_r, z_s, z_r, gz_s, gz_r, gx_s, gx_r, t_s, t_r,
):
    nkv = nx * nz
    me = lax.axis_index("kv")
    tp = lax.axis_index("tp")
    z_me, x_me = me // nx, me % nx
    width, rs = nb.shape[3], nb.shape[2]
    heads = xs.shape[0]
    dk = hgain_ref.shape[1]
    seqs_all, props = tok_ref.shape[0], tok_ref.shape[1]
    rows_all = seqs_all * props
    seqs = car_v.shape[0]
    nheads = wd_v.shape[1]
    dmodel = width * nkv

    loads = [
        pltpu.make_async_copy(src, w_v.at[i], loc.at[i]) for i, src in enumerate((wq_hbm, wk_hbm, wv_hbm, wz_hbm))
    ]
    mine = pl.ds(pl.multiple_of(me * width, width), width)
    loads.append(pltpu.make_async_copy(wd_hbm.at[mine], wd_v, loc.at[4]))
    loads.append(pltpu.make_async_copy(wb_hbm.at[mine], wb_v, loc.at[5]))
    late = [pltpu.make_async_copy(car_hbm, car_v, loc.at[6]), pltpu.make_async_copy(wo_hbm, wo_v, loc.at[7])]
    for load in loads + late:
        load.start()

    barrier = pltpu.get_barrier_semaphore()
    for r in range(1, nkv):
        pl.semaphore_signal(barrier, inc=1, device_id={"kv": lax.rem(me + r, nkv)}, device_id_type=MESH)
    for r in range(1, ntp):
        pl.semaphore_signal(barrier, inc=1, device_id={"tp": lax.rem(tp + r, ntp)}, device_id_type=MESH)

    for s in range(seqs_all):
        xrow[s * props : (s + 1) * props, :] = tok_ref[s].astype(f32)
    for d in range(nkv):
        part = xrow[d * rs : (d + 1) * rs, :]
        sq = jnp.sum(part * part, axis=1, keepdims=True)
        eye = lax.broadcasted_iota(jnp.int32, (rs, rs), 0) == lax.broadcasted_iota(jnp.int32, (rs, rs), 1)
        ssb[me, d : d + 1, 0:rs] = jnp.sum(jnp.where(eye, sq, 0.0), axis=0, keepdims=True)
    pl.semaphore_wait(barrier, nkv - 1 + ntp - 1)

    def kv_copy(src, dst, send, recv, kv):
        return pltpu.make_async_remote_copy(
            src_ref=src, dst_ref=dst, send_sem=send, recv_sem=recv, device_id={"kv": kv}, device_id_type=MESH
        )

    def ss_copy(r, slot):
        return kv_copy(ssb.at[me], ssb.at[slot], ss_s.at[r - 1], ss_r.at[r - 1], lax.rem(me + r, nkv))

    for r in range(1, nkv):
        ss_copy(r, me).start()
    for r in range(1, nkv):
        ss_copy(r, lax.rem(me - r + nkv, nkv)).wait_recv()
    total_sq = ssb[0]
    for d in range(1, nkv):
        total_sq = total_sq + ssb[d]
    gain = gain_ref[:, mine]
    for d in range(nkv):
        eye = lax.broadcasted_iota(jnp.int32, (rs, rs), 0) == lax.broadcasted_iota(jnp.int32, (rs, rs), 1)
        col = jnp.sum(jnp.where(eye, total_sq[d : d + 1, 0:rs], 0.0), axis=1, keepdims=True)
        scale = lax.rsqrt(col / dmodel + epsilon)
        nb[d // nx, d % nx] = (xrow[d * rs : (d + 1) * rs, :] * scale * gain).astype(bf16)
    for load in loads:
        load.wait()

    def x_copy(h, r):
        return kv_copy(xs.at[h, r - 1], xr.at[h, r - 1], x_s.at[h, r - 1], x_r.at[h, r - 1], z_me * nx + lax.rem(x_me + r, nx))

    def ax_copy(r):
        return kv_copy(axs.at[r - 1], axr.at[r - 1], x_s.at[heads, r - 1], x_r.at[heads, r - 1], z_me * nx + lax.rem(x_me + r, nx))

    def z_copy(h, r):
        to = lax.rem(z_me + r, nz)
        return kv_copy(zs.at[h, to], zr.at[h, r - 1], z_s.at[h, r - 1], z_r.at[h, r - 1], to * nx + x_me)

    def az_copy(r):
        to = lax.rem(z_me + r, nz)
        return kv_copy(azs.at[to], azr.at[r - 1], z_s.at[heads, r - 1], z_r.at[heads, r - 1], to * nx + x_me)

    def lanes(h):
        return pl.ds(pl.multiple_of(h * dk, dk), dk)

    def gz_copy(h, r, slot):
        here = gat.at[z_me, x_me, :, lanes(h)]
        there = gat.at[slot, x_me, :, lanes(h)]
        return kv_copy(here, there, gz_s.at[h, r - 1], gz_r.at[h, r - 1], lax.rem(z_me + r, nz) * nx + x_me)

    def gx_copy(h, r, slot):
        here = gat.at[:, x_me, :, lanes(h)]
        there = gat.at[:, slot, :, lanes(h)]
        return kv_copy(here, there, gx_s.at[h, r - 1], gx_r.at[h, r - 1], z_me * nx + lax.rem(x_me + r, nx))

    wab = jnp.concatenate([wd_v[...], wb_v[...], jnp.zeros((width, axs.shape[3] - 2 * nheads), bf16)], axis=1)
    for r in range(nx):
        rows = nb[:, lax.rem(x_me + r, nx)].reshape(nz * rs, width)
        got = fast_dot(rows, wab).reshape(nz, rs, -1)
        if r == 0:
            aown[...] = got
        else:
            axs[r - 1] = got.astype(bf16)
            ax_copy(r).start()

    @pl.loop(0, heads)
    def project(h):
        for r in list(range(1, nx)) + [0]:
            rows = nb[:, lax.rem(x_me + r, nx)].reshape(nz * rs, width)
            for i in range(4):
                got = fast_dot(rows, w_v[i, :, lanes(h)]).reshape(nz, rs, dk)
                at = slice(i * dk, (i + 1) * dk)
                if r == 0:
                    own[h, :, :, at] = got
                else:
                    xs[h, r - 1, :, :, at] = got.astype(bf16)
            if r > 0:
                x_copy(h, r).start()

    for r in range(1, nx):
        ax_copy(r).wait_recv()
        aown[...] += axr[r - 1].astype(f32)
    azs[...] = aown[...].astype(bf16)
    for r in range(1, nz):
        az_copy(r).start()

    late[0].wait()

    def stage_b(h):
        for r in range(1, nx):
            x_copy(h, r).wait_recv()
        pair = own[h]
        for r in range(1, nx):
            pair = pair + xr[h, r - 1].astype(f32)
        zs[h] = pair.astype(bf16)
        own[h] = pair
        for r in range(1, nz):
            z_copy(h, r).start()

    def stage_c(h):
        for r in range(1, nz):
            z_copy(h, r).wait_recv()
        tot = own[h, z_me]
        for r in range(1, nz):
            tot = tot + zr[h, r - 1].astype(f32)
        qraw, kraw, vraw, zraw = (tot[:, i * dk : (i + 1) * dk] for i in range(4))

        def unit(v):
            v = v * jax.nn.sigmoid(v)
            return v * lax.rsqrt(jnp.sum(v * v, axis=1, keepdims=True) + epsilon)

        query = unit(qraw) * dk ** (-0.5)
        key = unit(kraw)
        value = vraw * jax.nn.sigmoid(vraw)
        ab = abt[...]
        lane = lax.broadcasted_iota(jnp.int32, ab.shape, 1)
        head = tp * heads + h
        araw = jnp.sum(jnp.where(lane == head, ab, 0.0), axis=1, keepdims=True)
        braw = jnp.sum(jnp.where(lane == head + nheads, ab, 0.0), axis=1, keepdims=True)
        rate_lane = lax.broadcasted_iota(jnp.int32, rate_ref.shape, 1)
        rate = jnp.sum(jnp.where(rate_lane == head, rate_ref[...], 0.0), axis=1, keepdims=True)
        beta = jax.nn.sigmoid(braw)
        softplus = jnp.maximum(araw, 0.0) + jnp.log(1.0 + jnp.exp(-jnp.abs(araw)))
        g = -rate * softplus
        cum, decay, _, strict = chain(g, beta, key, props)
        x = jnp.concatenate([key, query], axis=0)
        prods = split_dot(x, key, ((1,), (1,)))
        a = jnp.where(strict, beta * decay * prods[:rs], 0.0)
        xh, xl = split(x)
        st = car_v[:, h].reshape(seqs * dk, -1)
        sh, sl = split(st)
        wide = spread_rows(xh, seqs, props)
        seen = fast_dot(wide, sh) + (fast_dot(spread_rows(xl, seqs, props), sh) + fast_dot(wide, sl))
        grow = jnp.exp(cum)
        u = solve(a, beta * (value - grow * seen[:rs]), props)
        att = grow * seen[rs:] + split_dot(decay * prods[rs:], u)
        ho = att * lax.rsqrt(jnp.mean(att * att, axis=1, keepdims=True) + epsilon)
        ho = ho * hgain_ref[...] * (zraw * jax.nn.sigmoid(zraw))
        gat[z_me, x_me, :, lanes(h)] = ho.astype(bf16)
        for r in range(1, nz):
            gz_copy(h, r, z_me).start()

    def stage_d(h):
        for r in range(1, nz):
            gz_copy(h, r, lax.rem(z_me - r + nz, nz)).wait_recv()
        for r in range(1, nx):
            gx_copy(h, r, x_me).start()

    lag_c, lag_d = 1, 2
    stage_b(0)
    for r in range(1, nz):
        az_copy(r).wait_recv()
    ab_total = aown[z_me]
    for r in range(1, nz):
        ab_total = ab_total + azr[r - 1].astype(f32)
    abt[...] = ab_total

    @pl.loop(1, heads + lag_d)
    def pipeline(i):
        @pl.when(i < heads)
        def _():
            stage_b(i)

        @pl.when((i >= lag_c) & (i < heads + lag_c))
        def _():
            stage_c(i - lag_c)

        @pl.when(i >= lag_d)
        def _():
            stage_d(i - lag_d)

    late[1].wait()

    @pl.loop(0, heads)
    def arrived(h):
        for r in range(1, nx):
            gx_copy(h, r, lax.rem(x_me - r + nx, nx)).wait_recv()

    share = rows_all // ntp

    def t_copy(r):
        to = lax.rem(tp + r, ntp)
        return pltpu.make_async_remote_copy(
            src_ref=ts.at[to], dst_ref=tr.at[r - 1], send_sem=t_s.at[r - 1], recv_sem=t_r.at[r - 1],
            device_id={"tp": to}, device_id_type=MESH,
        )

    got = fast_dot(gat[...].reshape(rows_all, -1), wo_v[...]).reshape(ntp, share, -1)
    terms[...] = got
    ts[...] = got.astype(bf16)
    for r in range(1, ntp):
        t_copy(r).start()
    for r in range(1, ntp):
        t_copy(r).wait_recv()
    result = terms[tp]
    for r in range(1, ntp):
        result = result + tr[r - 1].astype(f32)
    out_ref[...] = result.astype(bf16)

    for r in range(1, nkv):
        ss_copy(r, me).wait_send()
    for r in range(1, nx):
        ax_copy(r).wait_send()
    for r in range(1, nz):
        az_copy(r).wait_send()
    for r in range(1, ntp):
        t_copy(r).wait_send()

    @pl.loop(0, heads)
    def drain(h):
        for r in range(1, nx):
            x_copy(h, r).wait_send()
            gx_copy(h, r, x_me).wait_send()
        for r in range(1, nz):
            z_copy(h, r).wait_send()
            gz_copy(h, r, z_me).wait_send()


def step_call(nkv, ntp, tokens, norm_gain, wd, wb, rate, hgain, wq, wk, wv, wz, wo, carried):
    nx = 1
    while nx * nx * 4 <= nkv:
        nx *= 2
    nz = nkv // nx
    seqs, heads, dk, dv = carried.shape
    seqs_all, props, width = tokens.shape
    rs = seqs * props
    rows_all = seqs_all * props
    nheads = wd.shape[1]
    ab = -(-2 * nheads // 128) * 128
    out_cols = wo.shape[1]
    share = rows_all // ntp
    vmem = pl.BlockSpec(memory_space=pltpu.VMEM)
    anyw = pl.BlockSpec(memory_space=pl.ANY)
    V = pltpu.VMEM
    dma = pltpu.SemaphoreType.DMA
    return pl.pallas_call(
        functools.partial(step_kernel, nx, nz, ntp),
        out_shape=jax.ShapeDtypeStruct((share, out_cols), bf16),
        in_specs=[vmem, vmem, anyw, anyw, vmem, vmem] + [anyw] * 6,
        out_specs=vmem,
        scratch_shapes=[
            V((rows_all, width), f32),
            V((4,) + wq.shape, bf16),
            V(wo.shape, bf16),
            V((width, nheads), bf16),
            V((width, nheads), bf16),
            V(carried.shape, f32),
            V((nkv, nkv, 128), f32),
            V((nz, nx, rs, width), bf16),
            V((heads, nx - 1, nz, rs, 4 * dk), bf16),
            V((heads, nx - 1, nz, rs, 4 * dk), bf16),
            V((heads, nz, rs, 4 * dk), f32),
            V((heads, nz, rs, 4 * dk), bf16),
            V((heads, nz - 1, rs, 4 * dk), bf16),
            V((nx - 1, nz, rs, ab), bf16),
            V((nx - 1, nz, rs, ab), bf16),
            V((nz, rs, ab), f32),
            V((nz, rs, ab), bf16),
            V((nz - 1, rs, ab), bf16),
            V((rs, ab), f32),
            V((nz, nx, rs, heads * dv), bf16),
            V((ntp, share, out_cols), f32),
            V((ntp, share, out_cols), bf16),
            V((ntp - 1, share, out_cols), bf16),
            dma((8,)),
            dma((nkv - 1,)), dma((nkv - 1,)),
            dma((heads + 1, nx - 1)), dma((heads + 1, nx - 1)),
            dma((heads + 1, nz - 1)), dma((heads + 1, nz - 1)),
            dma((heads, nz - 1)), dma((heads, nz - 1)),
            dma((heads, nx - 1)), dma((heads, nx - 1)),
            dma((ntp - 1,)), dma((ntp - 1,)),
        ],
        compiler_params=pltpu.CompilerParams(
            collective_id=0, has_side_effects=True, vmem_limit_bytes=48 * 1024 * 1024
        ),
    )(tokens, norm_gain, wd, wb, rate, hgain, wq, wk, wv, wz, wo, carried)


def solution(mesh):
    nkv, ntp = mesh.shape["kv"], mesh.shape["tp"]

    def per_device(
        tokens, norm_gain, w_query, w_key, w_value, w_gate, w_decay, w_beta, decay_rate, head_gain, w_out,
        state, prev_keys, prev_values, prev_log_decay, prev_beta, accepted,
    ):
        carried = carried_call(state, prev_keys, prev_values, prev_log_decay, prev_beta, accepted)
        mixed = step_call(
            nkv, ntp, tokens, norm_gain.reshape(1, -1), w_decay, w_beta, decay_rate.reshape(1, -1),
            head_gain.reshape(1, -1), w_query, w_key, w_value, w_gate, w_out, carried,
        )
        return mixed.reshape(-1, tokens.shape[1], mixed.shape[1]), carried

    placed = (
        P(None, None, "kv"), P(), P("kv", "tp"), P("kv", "tp"), P("kv", "tp"), P("kv", "tp"), P(), P(), P(), P(),
        P("tp", "kv"), P("kv", "tp", None, None), P("kv", "tp", None, None), P("kv", "tp", None, None),
        P("kv", "tp", None), P("kv", "tp", None), P("kv"),
    )
    return jax.shard_map(
        per_device,
        mesh=mesh,
        in_specs=placed,
        out_specs=(P("tp", None, "kv"), P("kv", "tp", None, None)),
        check_vma=False,
    )
```

time: 256 us -> 80 us (0.31)
  waiting for transfers between devices: 85.9 us -> 0 us
  matrix products: 82.3 us -> 0 us
  Pallas kernels: 0 us -> 70 us
  blocking collectives: 44.4 us -> 0 us
  other arithmetic: 13.9 us -> 0 us
  between operations: 14.4 us -> 0.73 us
  local copies, waits for them, and re-layouts: 13.2 us -> 8.86 us
    reduce_scatter x2 -> x0, waiting for transfers between devices: 85.9 us -> none  [the longest x1 58.7 us: per_device(): lax.psum_scatter(jnp.dot(normed, joined, preferred_element_type=f32), 'kv...]
    dot_general x14 -> x0, matrix products: 82.3 us -> none  [the longest x8 47.3 us: apply_update(): jnp.einsum('bhde,bhd->bhe', decayed, keyvec, precision=lax.Precision.HIGH...]
    pallas_call x0 -> x2, Pallas kernels: none -> 70 us  [the longest x1 60 us: step_call(): pl.pallas_call(functools.partial(step_kernel, nx, nz, ntp), out_shape=jax...]
    all_gather x1 -> x0, blocking collectives: 25.7 us -> none  [per_device(): lax.all_gather(headout, 'kv', axis=0, tiled=True)]
    psum x1 -> x0, blocking collectives: 18.7 us -> none  [per_device(): total_sq = lax.psum(jnp.sum(features * features, axis=1), 'kv')]
    concatenate x1 -> x0, local copies, waits for them, and re-layouts: 7.62 us -> none  [per_device(): jnp.concatenate([w_query, w_key, w_value, w_gate, lax.dynamic_slice_in_di...]
    unnamed x23 -> x18, local copies, waits for them, and re-layouts: 0.78 us -> 8.21 us
    add x1 -> x0, other arithmetic: 6.66 us -> none  [apply_update(): decayed + jnp.einsum('bhd,bhe->bhde', keyvec, change, precision=lax.Preci...]
  transfers between devices with their start and end apart: 2 -> 0, of which waited for: 2 -> 0; matrix products, arithmetic and copies ran while one was open for 12% -> 0% of each run, Pallas kernels for 0% -> 0%
where the time goes in v1:
time: 80 us; the launch traced here: 79.6 us
  Pallas kernels  70 us (88%)
  local copies, waits for them, and re-layouts  8.86 us (11%)
    pallas_call x1, Pallas kernels, step_call(): pl.pallas_call(functools.partial(step_kernel, nx, nz, ntp), out_shape=jax...  60 us
    pallas_call x1, Pallas kernels, carried_call(): pl.pallas_call(carried_kernel, grid=(seqs // step,), out_shape=jax.ShapeD...  9.96 us
    unnamed x18, local copies, waits for them, and re-layouts  8.21 us

profile of v1, /device:TPU:1, one launch (start us, length us, event | category | flops | bytes accessed | tf_op | source)
XLA Modules:
  0.0 79.6 jit_solution(4992024835400137894)
XLA Ops:
  0.6 1.4 %copy.19.logd_ref = f32[8,8,4]{2,1,0:T(8,128)} copy(f32[8,8,4]{1,2,0:T(4,128)} %param.31) | data formatting | bytes 2048 | tf_op args[14]
  2.1 1.4 %copy.20.beta_ref = f32[8,8,4]{2,1,0:T(8,128)} copy(f32[8,8,4]{1,2,0:T(4,128)} %param.32) | data formatting | bytes 2048 | tf_op args[15]
  3.5 1.4 %copy.21.wd_hbm = bf16[4096,32]{1,0:T(8,128)(2,1)S(1)} copy(bf16[4096,32]{0,1:T(8,128)(2,1)} %param.23) | data formatting | bytes 524288 | tf_op args[6]
  4.9 1.4 %copy.22.wb_hbm = bf16[4096,32]{1,0:T(8,128)(2,1)S(1)} copy(bf16[4096,32]{0,1:T(8,128)(2,1)} %param.24) | data formatting | bytes 524288 | tf_op args[7]
  6.4 0.0 copy-start
  6.4 0.0 copy-start.3
  6.4 0.0 copy-start.4
  6.4 0.0 copy-start.5
  6.4 0.0 copy-start.6
  6.4 10.0 %shard_map.176.car_hbm = f32[8,8,128,128]{3,2,1,0:T(8,128)} custom-call(f32[8,8,128,128]{3,2,1,0:T(8,128)} %state_ref.1, bf16[8,8,4,128]{3,2,1,0:T(4,128)(2,1)} %keys_ref.1, bf16[8,8,4,128]{3,2,1,0:T(4,128)(2,1)} %values_ref.1, f32[8,8,4]{2,1,0:T(8,128)} %copy.19.logd_ref, f32[8,8,4]{2,1,0:T(8,128)} %copy.20.beta_ref, s32[8]{0:T(128)} %acc_ref.1), custom_call_target="tpu_custom_call" | custom-call | flops 8388608 | bytes 8388608 | tf_op jit(solution)/shard_map/pallas_call | solution.py:120
  16.4 0.0 copy-done
  16.4 0.0 copy-done.3
  16.4 0.0 copy-done.4
  16.4 0.0 copy-done.5
  16.4 0.0 copy-done.6
  16.4 0.0 copy-start.1
  16.5 1.2 %copy-done.1 = bf16[512,1024]{1,0:T(8,128)(2,1)S(1)} copy-done((bf16[512,1024]{1,0:T(8,128)(2,1)S(1)}, bf16[512,1024]{1,0:T(8,128)(2,1)}, u32[]{:S(2)}) %copy-start.1) | copy-done | bytes 1048600
  17.7 0.0 copy-start.2
  17.7 1.2 %copy-done.2 = bf16[512,1024]{1,0:T(8,128)(2,1)S(1)} copy-done((bf16[512,1024]{1,0:T(8,128)(2,1)S(1)}, bf16[512,1024]{1,0:T(8,128)(2,1)}, u32[]{:S(2)}) %copy-start.2) | copy-done | bytes 1048600
  18.9 60.0 %shard_map.177 = bf16[64,512]{1,0:T(8,128)(2,1)S(1)} custom-call(bf16[64,4,512]{2,1,0:T(4,128)(2,1)S(1)} %copy-done.3, f32[1,4096]{1,0:T(1,128)S(1)} %bitcast.3, bf16[4096,32]{1,0:T(8,128)(2,1)S(1)} %copy.21.wd_hbm, bf16[4096,32]{1,0:T(8,128)(2,1)S(1)} %copy.22.wb_hbm, f32[1,32]{1,0:T(1,128)S(1)} %bitcast.4, f32[1,128]{1,0:T(1,128)S(1)} %bitcast.5, ...), custom_call_target="tpu_custom_call" | custom-call | tf_op jit(solution)/shard_map/pallas_call | solution.py:414
  78.9 0.7 reshape.19
Async XLA Ops:
  6.4 10.0 %copy-start = (bf16[512,1024]{1,0:T(8,128)(2,1)S(1)}, bf16[512,1024]{1,0:T(8,128)(2,1)}, u32[]{:S(2)}) copy-start(bf16[512,1024]{1,0:T(8,128)(2,1)} %wq_hbm.1) | copy-start | bytes 3145732
  6.4 10.0 %copy-start.3 = (bf16[64,4,512]{2,1,0:T(4,128)(2,1)S(1)}, bf16[64,4,512]{2,1,0:T(4,128)(2,1)}, u32[]{:S(2)}) copy-start(bf16[64,4,512]{2,1,0:T(4,128)(2,1)} %tok_ref.1) | copy-start | bytes 786436
  6.4 10.0 %copy-start.4 = (f32[4096]{0:T(1024)S(1)}, f32[4096]{0:T(1024)}, u32[]{:S(2)}) copy-start(f32[4096]{0:T(1024)} %param.18) | copy-start | bytes 49156
  6.4 10.0 %copy-start.5 = (f32[32]{0:T(128)S(1)}, f32[32]{0:T(128)}, u32[]{:S(2)}) copy-start(f32[32]{0:T(128)} %param.25) | copy-start | bytes 388
  6.4 10.0 %copy-start.6 = (f32[128]{0:T(128)S(1)}, f32[128]{0:T(128)}, u32[]{:S(2)}) copy-start(f32[128]{0:T(128)} %param.26) | copy-start | bytes 1540
  16.4 1.2 %copy-start.1 = (bf16[512,1024]{1,0:T(8,128)(2,1)S(1)}, bf16[512,1024]{1,0:T(8,128)(2,1)}, u32[]{:S(2)}) copy-start(bf16[512,1024]{1,0:T(8,128)(2,1)} %wk_hbm.1) | copy-start | bytes 3145732
  17.7 1.2 %copy-start.2 = (bf16[512,1024]{1,0:T(8,128)(2,1)S(1)}, bf16[512,1024]{1,0:T(8,128)(2,1)}, u32[]{:S(2)}) copy-start(bf16[512,1024]{1,0:T(8,128)(2,1)} %wv_hbm.1) | copy-start | bytes 3145732

commit v2 on v1

--- a/solution.py
+++ b/solution.py
@@ -86,8 +86,8 @@
             vrow[s, h * props : (h + 1) * props, :] = values_ref[s, h].astype(f32)
     for s in range(seqs):
         keep = prop_of < acc_ref[first + s]
-        g = jnp.sum(jnp.where(pick, exact_dot(repeat, logd_ref[s]), 0.0), axis=1, keepdims=True)
-        b = jnp.sum(jnp.where(pick, exact_dot(repeat, beta_ref[s]), 0.0), axis=1, keepdims=True)
+        g = jnp.sum(jnp.where(pick, exact_dot(repeat, logd_ref[s], ((1,), (1,))), 0.0), axis=1, keepdims=True)
+        b = jnp.sum(jnp.where(pick, exact_dot(repeat, beta_ref[s], ((1,), (1,))), 0.0), axis=1, keepdims=True)
         g = jnp.where(keep, g, 0.0)
         b = jnp.where(keep, b, 0.0)
         key = krow[s]
@@ -114,7 +114,7 @@
 def carried_call(state, prev_keys, prev_values, prev_log_decay, prev_beta, accepted):
     seqs, heads, dk, dv = state.shape
     props = prev_keys.shape[2]
-    step = 2 if seqs % 2 == 0 else 1
+    step = 4 if seqs % 4 == 0 else 1
     at4 = lambda i: (i, 0, 0, 0)
     at3 = lambda i: (i, 0, 0)
     return pl.pallas_call(
@@ -125,8 +125,8 @@
             pl.BlockSpec((step, heads, dk, dv), at4),
             pl.BlockSpec((step, heads, props, dk), at4),
             pl.BlockSpec((step, heads, props, dv), at4),
-            pl.BlockSpec((step, heads, props), at3),
-            pl.BlockSpec((step, heads, props), at3),
+            pl.BlockSpec((step, props, heads), at3),
+            pl.BlockSpec((step, props, heads), at3),
             pl.BlockSpec(memory_space=pltpu.SMEM),
         ],
         out_specs=pl.BlockSpec((step, heads, dk, dv), at4),
@@ -152,17 +152,17 @@
     seqs_all, props = tok_ref.shape[0], tok_ref.shape[1]
     rows_all = seqs_all * props
     seqs = car_v.shape[0]
-    nheads = wd_v.shape[1]
+    nheads = wd_v.shape[0]
     dmodel = width * nkv
 
     loads = [
         pltpu.make_async_copy(src, w_v.at[i], loc.at[i]) for i, src in enumerate((wq_hbm, wk_hbm, wv_hbm, wz_hbm))
     ]
     mine = pl.ds(pl.multiple_of(me * width, width), width)
-    loads.append(pltpu.make_async_copy(wd_hbm.at[mine], wd_v, loc.at[4]))
-    loads.append(pltpu.make_async_copy(wb_hbm.at[mine], wb_v, loc.at[5]))
+    loads.append(pltpu.make_async_copy(wd_hbm.at[:, mine], wd_v, loc.at[4]))
+    loads.append(pltpu.make_async_copy(wb_hbm.at[:, mine], wb_v, loc.at[5]))
     late = [pltpu.make_async_copy(car_hbm, car_v, loc.at[6]), pltpu.make_async_copy(wo_hbm, wo_v, loc.at[7])]
-    for load in loads + late:
+    for load in loads:
         load.start()
 
     barrier = pltpu.get_barrier_semaphore()
@@ -203,6 +203,8 @@
         nb[d // nx, d % nx] = (xrow[d * rs : (d + 1) * rs, :] * scale * gain).astype(bf16)
     for load in loads:
         load.wait()
+    for load in late:
+        load.start()
 
     def x_copy(h, r):
         return kv_copy(xs.at[h, r - 1], xr.at[h, r - 1], x_s.at[h, r - 1], x_r.at[h, r - 1], z_me * nx + lax.rem(x_me + r, nx))
@@ -222,19 +224,19 @@
         return pl.ds(pl.multiple_of(h * dk, dk), dk)
 
     def gz_copy(h, r, slot):
-        here = gat.at[z_me, x_me, :, lanes(h)]
-        there = gat.at[slot, x_me, :, lanes(h)]
+        here = gat.at[h, x_me, z_me]
+        there = gat.at[h, x_me, slot]
         return kv_copy(here, there, gz_s.at[h, r - 1], gz_r.at[h, r - 1], lax.rem(z_me + r, nz) * nx + x_me)
 
     def gx_copy(h, r, slot):
-        here = gat.at[:, x_me, :, lanes(h)]
-        there = gat.at[:, slot, :, lanes(h)]
+        here = gat.at[h, x_me]
+        there = gat.at[h, slot]
         return kv_copy(here, there, gx_s.at[h, r - 1], gx_r.at[h, r - 1], z_me * nx + lax.rem(x_me + r, nx))
 
-    wab = jnp.concatenate([wd_v[...], wb_v[...], jnp.zeros((width, axs.shape[3] - 2 * nheads), bf16)], axis=1)
+    wab = jnp.concatenate([wd_v[...], wb_v[...], jnp.zeros((axs.shape[3] - 2 * nheads, width), bf16)], axis=0)
     for r in range(nx):
         rows = nb[:, lax.rem(x_me + r, nx)].reshape(nz * rs, width)
-        got = fast_dot(rows, wab).reshape(nz, rs, -1)
+        got = fast_dot(rows, wab, ((1,), (1,))).reshape(nz, rs, -1)
         if r == 0:
             aown[...] = got
         else:
@@ -310,11 +312,17 @@
         wide = spread_rows(xh, seqs, props)
         seen = fast_dot(wide, sh) + (fast_dot(spread_rows(xl, seqs, props), sh) + fast_dot(wide, sl))
         grow = jnp.exp(cum)
-        u = solve(a, beta * (value - grow * seen[:rs]), props)
-        att = grow * seen[rs:] + split_dot(decay * prods[rs:], u)
+        reads = decay * prods[rs:]
+        reads = reads - split_dot(reads, a)
+        power, reach = a, 2
+        while reach < props:
+            power = split_dot(power, power)
+            reads = reads + split_dot(reads, power)
+            reach *= 2
+        att = grow * seen[rs:] + split_dot(reads, beta * (value - grow * seen[:rs]))
         ho = att * lax.rsqrt(jnp.mean(att * att, axis=1, keepdims=True) + epsilon)
         ho = ho * hgain_ref[...] * (zraw * jax.nn.sigmoid(zraw))
-        gat[z_me, x_me, :, lanes(h)] = ho.astype(bf16)
+        gat[h, x_me, z_me] = ho.astype(bf16)
         for r in range(1, nz):
             gz_copy(h, r, z_me).start()
 
@@ -324,7 +332,7 @@
         for r in range(1, nx):
             gx_copy(h, r, x_me).start()
 
-    lag_c, lag_d = 1, 2
+    lag_c, lag_d = 2, 4
     stage_b(0)
     for r in range(1, nz):
         az_copy(r).wait_recv()
@@ -363,7 +371,14 @@
             device_id={"tp": to}, device_id_type=MESH,
         )
 
-    got = fast_dot(gat[...].reshape(rows_all, -1), wo_v[...]).reshape(ntp, share, -1)
+    left = jnp.concatenate(
+        [
+            jnp.concatenate([gat[h, d % nx, d // nx] for d in range(nkv)], axis=0)
+            for h in range(heads)
+        ],
+        axis=1,
+    )
+    got = fast_dot(left, wo_v[...]).reshape(ntp, share, -1)
     terms[...] = got
     ts[...] = got.astype(bf16)
     for r in range(1, ntp):
@@ -403,12 +418,12 @@
     seqs_all, props, width = tokens.shape
     rs = seqs * props
     rows_all = seqs_all * props
-    nheads = wd.shape[1]
+    nheads = wd.shape[0]
     ab = -(-2 * nheads // 128) * 128
     out_cols = wo.shape[1]
     share = rows_all // ntp
     vmem = pl.BlockSpec(memory_space=pltpu.VMEM)
-    anyw = pl.BlockSpec(memory_space=pl.ANY)
+    anyw = pl.BlockSpec(memory_space=pltpu.HBM)
     V = pltpu.VMEM
     dma = pltpu.SemaphoreType.DMA
     return pl.pallas_call(
@@ -420,8 +435,8 @@
             V((rows_all, width), f32),
             V((4,) + wq.shape, bf16),
             V(wo.shape, bf16),
-            V((width, nheads), bf16),
-            V((width, nheads), bf16),
+            V((nheads, width), bf16),
+            V((nheads, width), bf16),
             V(carried.shape, f32),
             V((nkv, nkv, 128), f32),
             V((nz, nx, rs, width), bf16),
@@ -436,7 +451,7 @@
             V((nz, rs, ab), bf16),
             V((nz - 1, rs, ab), bf16),
             V((rs, ab), f32),
-            V((nz, nx, rs, heads * dv), bf16),
+            V((heads, nx, nz, rs, dv), bf16),
             V((ntp, share, out_cols), f32),
             V((ntp, share, out_cols), bf16),
             V((ntp - 1, share, out_cols), bf16),
@@ -449,7 +464,7 @@
             dma((ntp - 1,)), dma((ntp - 1,)),
         ],
         compiler_params=pltpu.CompilerParams(
-            collective_id=0, has_side_effects=True, vmem_limit_bytes=48 * 1024 * 1024
+            collective_id=0, has_side_effects=True, vmem_limit_bytes=62 * 1024 * 1024
         ),
     )(tokens, norm_gain, wd, wb, rate, hgain, wq, wk, wv, wz, wo, carried)
 
@@ -461,9 +476,11 @@
         tokens, norm_gain, w_query, w_key, w_value, w_gate, w_decay, w_beta, decay_rate, head_gain, w_out,
         state, prev_keys, prev_values, prev_log_decay, prev_beta, accepted,
     ):
-        carried = carried_call(state, prev_keys, prev_values, prev_log_decay, prev_beta, accepted)
+        carried = carried_call(
+            state, prev_keys, prev_values, prev_log_decay.transpose(0, 2, 1), prev_beta.transpose(0, 2, 1), accepted
+        )
         mixed = step_call(
-            nkv, ntp, tokens, norm_gain.reshape(1, -1), w_decay, w_beta, decay_rate.reshape(1, -1),
+            nkv, ntp, tokens, norm_gain.reshape(1, -1), w_decay.T, w_beta.T, decay_rate.reshape(1, -1),
             head_gain.reshape(1, -1), w_query, w_key, w_value, w_gate, w_out, carried,
         )
         return mixed.reshape(-1, tokens.shape[1], mixed.shape[1]), carried

time: 80 us -> 69.7 us (0.87)
  local copies, waits for them, and re-layouts: 8.86 us -> 1.49 us
  Pallas kernels: 70 us -> 67.4 us
    unnamed x18 -> x0, local copies, waits for them, and re-layouts: 8.21 us -> none
    pallas_call x1, Pallas kernels: 60 us -> 58 us  [step_call(): pl.pallas_call(functools.partial(step_kernel, nx, nz, ntp), out_shape=jax...]
    reshape x1, local copies, waits for them, and re-layouts: 0.65 us -> 1.49 us  [per_device(): return (mixed.reshape(-1, tokens.shape[1], mixed.shape[1]), carried)]
where the time goes in v2:
time: 69.7 us; the launch traced here: 69.6 us
  Pallas kernels  67.4 us (97%)
  local copies, waits for them, and re-layouts  1.49 us (2%)
    pallas_call x1, Pallas kernels, step_call(): pl.pallas_call(functools.partial(step_kernel, nx, nz, ntp), out_shape=jax...  58 us
    pallas_call x1, Pallas kernels, carried_call(): pl.pallas_call(carried_kernel, grid=(seqs // step,), out_shape=jax.ShapeD...  9.43 us
    reshape x1, local copies, waits for them, and re-layouts, per_device(): return (mixed.reshape(-1, tokens.shape[1], mixed.shape[1]), carried)  1.49 us

profile of v2, /device:TPU:1, one launch (start us, length us, event | category | flops | bytes accessed | tf_op | source)
XLA Modules:
  0.0 69.6 jit_solution(12728259536399634657)
XLA Ops:
  0.6 9.4 %shard_map.176.car_hbm = f32[8,8,128,128]{3,2,1,0:T(8,128)} custom-call(f32[8,8,128,128]{3,2,1,0:T(8,128)} %state_ref.1, bf16[8,8,4,128]{3,2,1,0:T(4,128)(2,1)} %keys_ref.1, bf16[8,8,4,128]{3,2,1,0:T(4,128)(2,1)} %values_ref.1, f32[8,4,8]{2,1,0:T(4,128)} %bitcast.9, f32[8,4,8]{2,1,0:T(4,128)} %bitcast.10, s32[8]{0:T(128)} %acc_ref.1), custom_call_target="tpu_custom_call" | custom-call | flops 8388608 | bytes 8388608 | tf_op jit(solution)/shard_map/pallas_call | solution.py:120
  10.1 58.0 %shard_map.177 = bf16[64,512]{1,0:T(8,128)(2,1)} custom-call(bf16[64,4,512]{2,1,0:T(4,128)(2,1)} %tok_ref.1, f32[1,4096]{1,0:T(1,128)} %bitcast.11, bf16[32,4096]{1,0:T(8,128)(2,1)} %bitcast.7, bf16[32,4096]{1,0:T(8,128)(2,1)} %bitcast.8, f32[1,32]{1,0:T(1,128)} %bitcast.12, f32[1,128]{1,0:T(1,128)} %bitcast.13, bf16[512,1024]{1,0:T(8,128)(2,1)} %wq_hbm.1, ...), custom_call_target="tpu_custom_call" | custom-call | tf_op jit(solution)/shard_map/pallas_call | solution.py:429
  68.1 1.5 %reshape.19 = bf16[16,4,512]{2,1,0:T(4,128)(2,1)} reshape(bf16[64,512]{1,0:T(8,128)(2,1)} %shard_map.177) | data formatting | bytes 131072 | tf_op jit(solution)/shard_map/reshape | solution.py:486
